TPU v7x, 32 devices: a whole 2x2x4 slice. The times are simulated.
32 devices in a mesh: sp: 16 (over z, y, x), tp: 2 (over core).
Axes of the slice: x: 2, y: 2, z: 4, core: 2. Of those that a mesh axis runs over, the one named last changes fastest.
Arguments:
- mixer_output: bfloat16 [2048, 2048], P('sp'), may hold values from -6 to 6
- layer_cotangent: bfloat16 [2048, 2048], P('sp'), may hold values from -6 to 6
- expert_choice: int32 [2048, 2], P('sp'), may hold values from 0 to 15, all different within a row; in each aligned block of 128 rows (0 to 127, 128 to 255, ...) at most 32 rows name the same one
- route_weight: float32 [2048, 2], P('sp'), may hold values from 0.1 to 0.9
- gate_pre: bfloat16 [16, 512, 1024], P('sp', None, 'tp'), may hold values from -15 to 15
- up_pre: bfloat16 [16, 512, 1024], P('sp', None, 'tp'), may hold values from -15 to 15
- w_gate: bfloat16 [16, 2048, 1024], P('sp', None, 'tp'), may hold values from -0.125 to 0.125
- w_up: bfloat16 [16, 2048, 1024], P('sp', None, 'tp'), may hold values from -0.125 to 0.125
- w_down: bfloat16 [16, 1024, 2048], P('sp', 'tp'), may hold values from -0.1875 to 0.1875
- w_out: bfloat16 [2048, 2048], P('tp'), may hold values from -0.125 to 0.125
- norm_gain: bfloat16 [2048], P('tp'), may hold values from 0.099609375 to 1.8984375
- scan_in: bfloat16 [2048, 2048], P('sp', 'tp'), may hold values from -6 to 6
- gate_in: bfloat16 [2048, 2048], P('sp', 'tp'), may hold values from -9 to 9
- b_proj: bfloat16 [2048, 1024], P('sp', 'tp'), may hold values from -1.796875 to 1.796875
- c_proj: bfloat16 [2048, 1024], P('sp', 'tp'), may hold values from -1.796875 to 1.796875
- log_decay: float32 [2048, 32], P('sp', 'tp'), may hold values from -3 to 0
- entry_state: float32 [16, 32, 64, 128], P('sp', 'tp'), may hold values from -24 to 24
Outputs:
- grad_w_gate: bfloat16 [16, 2048, 1024], P('sp', None, 'tp')
- grad_w_up: bfloat16 [16, 2048, 1024], P('sp', None, 'tp')
- grad_w_down: bfloat16 [16, 1024, 2048], P('sp', 'tp')
- grad_out_proj: float32 [2048, 2048], P('sp', 'tp')
- grad_scan_in: bfloat16 [2048, 2048], P('sp', 'tp')
- grad_gate_in: bfloat16 [2048, 2048], P('sp', 'tp')
- grad_b_proj: bfloat16 [2048, 1024], P('sp', 'tp')
- grad_c_proj: bfloat16 [2048, 1024], P('sp', 'tp')
- grad_log_decay: float32 [2048, 32], P('sp', 'tp')
Inputs may be any that keep to these rules, and one draw needn't show every extreme that they name: `expert_choice`: in the 128 rows of one device no expert is named more than 32 times, a bound that some blocks reach; the 2 entries of a row differ.
All inputs are finite; a program needn't handle non-finite values.
Results may differ from a plain program's by a relative error of at most 0.012.
Values may be sent and summed in bfloat16 or wider, within the bound.
A program may use at most 192 MiB of HBM per device.

v0:
```python
import jax
import jax.numpy as jnp
from jax import lax
from jax.sharding import PartitionSpec as P

HEAD_DIM = 64
STATE = 128
rms_epsilon = 1e-05
clamp_limit = 7.0
swish_alpha = 1.702


def entry_slots(expert_choice, expert_count, capacity):
    tokens, top_count = expert_choice.shape
    targets = expert_choice.reshape(-1)
    experts = jnp.arange(expert_count, dtype=jnp.int32)
    one_hot = (targets[:, None] == experts[None, :]).astype(jnp.float32)
    entries = jnp.arange(tokens * top_count, dtype=jnp.int32)
    before = (entries[:, None] > entries[None, :]).astype(jnp.bfloat16)
    earlier = jnp.dot(before, one_hot.astype(jnp.bfloat16), preferred_element_type=jnp.float32)
    ranks = jnp.sum(earlier * one_hot, axis=1).astype(jnp.int32)
    return (targets * capacity + ranks).reshape(tokens, top_count)


def expert_side(grad_rows, gate_value, up_value, gate_weight, up_weight, down_weight):
    act_grad = jnp.einsum("rd,fd->rf", grad_rows, down_weight, preferred_element_type=jnp.float32)
    gate_full = gate_value.astype(jnp.float32)
    up_full = up_value.astype(jnp.float32)
    gate_clip = jnp.minimum(gate_full, clamp_limit)
    up_clip = jnp.clip(up_full, -clamp_limit, clamp_limit)
    sigmoid_gate = jax.nn.sigmoid(swish_alpha * gate_clip)
    swish_gate = gate_clip * sigmoid_gate
    active = ((up_clip + 1.0) * swish_gate).astype(jnp.bfloat16)
    up_grad = jnp.where(
        (up_full > -clamp_limit) & (up_full < clamp_limit), act_grad * swish_gate, 0.0
    ).astype(jnp.bfloat16)
    slope = sigmoid_gate + swish_alpha * gate_clip * sigmoid_gate * (1.0 - sigmoid_gate)
    gate_grad = jnp.where(gate_full < clamp_limit, act_grad * (up_clip + 1.0) * slope, 0.0).astype(
        jnp.bfloat16
    )
    partial_rows = jnp.einsum(
        "rf,df->rd", gate_grad, gate_weight, preferred_element_type=jnp.float32
    )
    partial_rows = partial_rows + jnp.einsum(
        "rf,df->rd", up_grad, up_weight, preferred_element_type=jnp.float32
    )
    return (active, gate_grad, up_grad, partial_rows)


def exchange(pieces):
    return lax.all_to_all(pieces, "sp", split_axis=0, concat_axis=0, tiled=True)


def tell_all(vector):
    return exchange(jnp.broadcast_to(vector, (lax.axis_size("sp"), *vector.shape)))


def later_states(block_state, totals):
    count = lax.axis_size("sp")
    heads, channels, width = block_state.shape
    rows = heads * channels // count
    spots = jnp.arange(count)
    between = (
        (spots[:, None, None] < spots[None, None, :])
        & (spots[None, None, :] < spots[None, :, None])
    ).astype(jnp.float32)
    gaps = jnp.einsum("bck,kh->bch", between, totals, precision=lax.Precision.HIGHEST)
    later = spots[:, None, None] < spots[None, :, None]
    weights = jnp.where(later, jnp.exp(gaps), 0.0)
    first = lax.axis_index("sp") * rows
    picks = (
        ((first + jnp.arange(rows)) // channels)[None, :] == jnp.arange(heads)[:, None]
    ).astype(jnp.float32)
    weights = jnp.einsum("bch,hr->bcr", weights, picks, precision=lax.Precision.HIGHEST)
    dealt = lax.all_to_all(
        block_state.astype(jnp.bfloat16).reshape(count, rows, width),
        "sp",
        split_axis=0,
        concat_axis=0,
        tiled=True,
    ).astype(jnp.float32)
    sums = jnp.sum(weights[:, :, :, None] * dealt[None], axis=1)
    back = lax.all_to_all(sums.astype(jnp.bfloat16), "sp", split_axis=0, concat_axis=0, tiled=True)
    return back.reshape(heads, channels, width)


def body(
    mixer_output,
    layer_cotangent,
    expert_choice,
    route_weight,
    gate_pre,
    up_pre,
    w_gate,
    w_up,
    w_down,
    w_out,
    norm_gain,
    scan_in,
    gate_in,
    b_proj,
    c_proj,
    log_decay,
    entry_state,
):
    expert_count = lax.axis_size("sp")
    tokens_here = mixer_output.shape[0]
    model_width = mixer_output.shape[1]
    top_count = expert_choice.shape[1]
    capacity = gate_pre.shape[1] // expert_count
    columns = model_width // lax.axis_size("tp")
    first_column = lax.axis_index("tp") * columns
    own_cotangent = lax.dynamic_slice_in_dim(layer_cotangent, first_column, columns, 1).astype(
        jnp.float32
    )
    own_hidden = lax.dynamic_slice_in_dim(mixer_output, first_column, columns, 1)
    slots = entry_slots(expert_choice, expert_count, capacity)
    slot_ids = jnp.arange(expert_count * capacity, dtype=jnp.int32)
    places = (slots.T[:, None, :] == slot_ids[None, :, None]).astype(jnp.bfloat16)
    token_places = places.sum(axis=0)
    weighted = (route_weight.T[:, :, None] * own_cotangent[None]).astype(jnp.bfloat16)

    def dispatch(rows):
        arrived = lax.all_to_all(
            rows.astype(jnp.bfloat16).reshape(expert_count, capacity, columns),
            "sp",
            split_axis=0,
            concat_axis=0,
            tiled=True,
        ).reshape(-1, columns)
        return lax.all_gather(arrived, "tp", axis=1, tiled=True)

    recv_grads = dispatch(
        jnp.einsum("kst,ktd->sd", places, weighted, preferred_element_type=jnp.float32)
    )
    active, gate_grad, up_grad, partial_rows = expert_side(
        recv_grads, gate_pre[0], up_pre[0], w_gate[0], w_up[0], w_down[0]
    )
    summed = lax.psum_scatter(
        partial_rows.astype(jnp.bfloat16), "tp", scatter_dimension=1, tiled=True
    )
    returned = lax.all_to_all(
        summed.reshape(expert_count, capacity, -1), "sp", split_axis=0, concat_axis=0, tiled=True
    )
    head_count = log_decay.shape[1]
    group_count = b_proj.shape[1] // STATE
    per_group = head_count // group_count
    scan_heads = scan_in.reshape(tokens_here, head_count, HEAD_DIM)
    b_groups = b_proj.reshape(tokens_here, group_count, STATE)
    c_groups = c_proj.reshape(tokens_here, group_count, STATE)
    x_float = scan_heads.astype(jnp.float32)
    token_locations = jnp.arange(tokens_here)
    causal = token_locations[:, None] >= token_locations[None, :]
    causal_float = causal.astype(jnp.float32)
    cumulative = jnp.dot(causal_float, log_decay, precision=lax.Precision.HIGHEST)
    growth = jnp.exp(cumulative)
    block_decays = tell_all(lax.optimization_barrier((cumulative[-1], summed))[0])
    tail_decay = jnp.exp(cumulative[-1][None, :] - cumulative)
    log_gaps = cumulative.T[:, :, None] - cumulative.T[:, None, :]
    decay_mat = jnp.exp(jnp.where(causal[None], log_gaps, -jnp.inf))
    inner_prod = jnp.einsum("tgn,sgn->gts", c_groups, b_groups, preferred_element_type=jnp.float32)
    mix_weights = (jnp.repeat(inner_prod, per_group, axis=0) * decay_mat).astype(jnp.bfloat16)
    state_groups = entry_state.astype(jnp.bfloat16).reshape(group_count, per_group, HEAD_DIM, STATE)
    y_inner = jnp.einsum(
        "hts,shp->thp", mix_weights, scan_heads, preferred_element_type=jnp.float32
    )
    y_carry = jnp.einsum(
        "tgn,grpn->tgrp", c_groups, state_groups, preferred_element_type=jnp.float32
    ).reshape(tokens_here, head_count, HEAD_DIM)
    scan_out = y_inner + y_carry * growth[:, :, None]
    gate_float = gate_in.astype(jnp.float32)
    gate_sig = jax.nn.sigmoid(gate_float)
    gate_silu = gate_float * gate_sig
    gated = scan_out.reshape(tokens_here, -1) * gate_silu
    grouped = gated.reshape(tokens_here, group_count, -1)
    inv_rms = lax.rsqrt(jnp.mean(grouped * grouped, axis=-1, keepdims=True) + rms_epsilon)
    unit = grouped * inv_rms
    gain_groups = norm_gain.astype(jnp.float32).reshape(group_count, -1)
    mixed = (unit * gain_groups).reshape(tokens_here, -1).astype(jnp.bfloat16)
    all_mixed = lax.all_gather(mixed, "sp", axis=0, tiled=True)
    returned, mixed = lax.optimization_barrier((returned, mixed))
    moe_terms = jnp.einsum(
        "st,sd->td", token_places, returned.reshape(-1, columns), preferred_element_type=jnp.float32
    )
    grad_hidden = lax.all_gather(
        (own_cotangent + moe_terms).astype(jnp.bfloat16), "tp", axis=1, tiled=True
    )
    late_hidden, grad_hidden = lax.optimization_barrier((own_hidden, grad_hidden))
    recv_hidden = dispatch(
        jnp.einsum("st,td->sd", token_places, late_hidden, preferred_element_type=jnp.float32)
    )
    down_wgrad = jnp.einsum(
        "rf,rd->fd", active, recv_grads, preferred_element_type=jnp.float32
    ).astype(jnp.bfloat16)
    gate_wgrad = jnp.einsum(
        "rd,rf->df", recv_hidden, gate_grad, preferred_element_type=jnp.float32
    ).astype(jnp.bfloat16)
    up_wgrad = jnp.einsum(
        "rd,rf->df", recv_hidden, up_grad, preferred_element_type=jnp.float32
    ).astype(jnp.bfloat16)
    own_block = lax.all_to_all(
        grad_hidden.reshape(tokens_here, expert_count, -1).transpose(1, 0, 2),
        "sp",
        split_axis=0,
        concat_axis=0,
        tiled=True,
    )
    grad_out_proj = jnp.einsum(
        "td,ti->di",
        own_block.reshape(-1, own_block.shape[2]),
        all_mixed,
        preferred_element_type=jnp.float32,
    )
    grad_mixed = jnp.einsum("td,id->ti", grad_hidden, w_out, preferred_element_type=jnp.float32)
    grad_unit = grad_mixed.reshape(tokens_here, group_count, -1) * gain_groups
    grad_grouped = inv_rms * (grad_unit - unit * jnp.mean(grad_unit * unit, axis=-1, keepdims=True))
    grad_gated = grad_grouped.reshape(tokens_here, -1)
    grad_gate_in = (
        grad_gated
        * scan_out.reshape(tokens_here, -1)
        * gate_sig
        * (1.0 + gate_float * (1.0 - gate_sig))
    ).astype(jnp.bfloat16)
    grad_y = (grad_gated * gate_silu).reshape(tokens_here, head_count, HEAD_DIM)
    grad_y_b = grad_y.astype(jnp.bfloat16)
    grad_x_inner = jnp.einsum(
        "hts,thp->shp", mix_weights, grad_y_b, preferred_element_type=jnp.float32
    )
    grad_weights = (
        jnp.einsum("thp,shp->hts", grad_y_b, scan_heads, preferred_element_type=jnp.float32)
        * decay_mat
    )
    grad_weights = (
        grad_weights.reshape(group_count, per_group, tokens_here, tokens_here)
        .sum(axis=1)
        .astype(jnp.bfloat16)
    )
    grad_c_inner = jnp.einsum(
        "gts,sgn->tgn", grad_weights, b_groups, preferred_element_type=jnp.float32
    )
    grad_b_inner = jnp.einsum(
        "gts,tgn->sgn", grad_weights, c_groups, preferred_element_type=jnp.float32
    )
    grown_grads = (
        (grad_y * growth[:, :, None])
        .astype(jnp.bfloat16)
        .reshape(tokens_here, group_count, per_group, HEAD_DIM)
    )
    grad_c_carry = jnp.einsum(
        "tgrp,grpn->tgn", grown_grads, state_groups, preferred_element_type=jnp.float32
    )
    block_state = jnp.einsum(
        "tgrp,tgn->grpn", grown_grads, c_groups, preferred_element_type=jnp.float32
    ).reshape(head_count, HEAD_DIM, STATE)
    x_tail = (
        (x_float * tail_decay[:, :, None])
        .astype(jnp.bfloat16)
        .reshape(tokens_here, group_count, per_group, HEAD_DIM)
    )
    later_state = later_states(block_state, block_decays)
    later_groups = later_state.reshape(group_count, per_group, HEAD_DIM, STATE)
    grad_x_carry = jnp.einsum(
        "sgn,grpn->sgrp", b_groups, later_groups, preferred_element_type=jnp.float32
    ).reshape(tokens_here, head_count, HEAD_DIM)
    grad_x = grad_x_inner + grad_x_carry * tail_decay[:, :, None]
    grad_b_carry = jnp.einsum(
        "sgrp,grpn->sgn", x_tail, later_groups, preferred_element_type=jnp.float32
    )
    grad_a = jnp.sum(grad_y * scan_out, axis=2) - jnp.sum(x_float * grad_x, axis=2)
    block_totals = tell_all(jnp.sum(grad_a, axis=0))
    is_later = jnp.arange(expert_count) > lax.axis_index("sp")
    later_grad = jnp.sum(jnp.where(is_later[:, None], block_totals, 0.0), axis=0)
    grad_log_decay = (
        jnp.dot(causal_float.T, grad_a, precision=lax.Precision.HIGHEST) + later_grad[None, :]
    )
    grad_scan_in = grad_x.reshape(tokens_here, -1).astype(jnp.bfloat16)
    grad_b_proj = (grad_b_inner + grad_b_carry).reshape(tokens_here, -1).astype(jnp.bfloat16)
    grad_c_proj = (grad_c_inner + grad_c_carry).reshape(tokens_here, -1).astype(jnp.bfloat16)
    return (
        gate_wgrad[None],
        up_wgrad[None],
        down_wgrad[None],
        grad_out_proj,
        grad_scan_in,
        grad_gate_in,
        grad_b_proj,
        grad_c_proj,
        grad_log_decay,
    )


def solution(mesh):
    in_specs = (
        P("sp", None),
        P("sp", None),
        P("sp", None),
        P("sp", None),
        P("sp", None, "tp"),
        P("sp", None, "tp"),
        P("sp", None, "tp"),
        P("sp", None, "tp"),
        P("sp", "tp", None),
        P("tp", None),
        P("tp"),
        P("sp", "tp"),
        P("sp", "tp"),
        P("sp", "tp"),
        P("sp", "tp"),
        P("sp", "tp"),
        P("sp", "tp", None, None),
    )
    out_specs = (
        P("sp", None, "tp"),
        P("sp", None, "tp"),
        P("sp", "tp", None),
        P("sp", "tp"),
        P("sp", "tp"),
        P("sp", "tp"),
        P("sp", "tp"),
        P("sp", "tp"),
        P("sp", "tp"),
    )
    return jax.shard_map(body, mesh=mesh, in_specs=in_specs, out_specs=out_specs, check_vma=False)
```

profile of v0, /device:TPU:0, one launch (start us, length us, event | category | flops | bytes accessed | tf_op | source)
XLA Modules:
  0.0 248.3 jit_solution(7997684214962049168)
XLA Ops:
  12.6 34.6 %all_to_all.48 = bf16[16,32,1024]{2,1,0:T(8,128)(2,1)} all-to-all(bf16[16,32,1024]{2,1,0:T(8,128)(2,1)S(1)} %bitcast.204), channel_id=1, replica_groups=mesh['sp'=16,'tp'=2] {'sp'}, dimensions={0} | all-to-all | bytes 2097152 | tf_op jit(solution)/shard_map/all_to_all | solution.py:124
  47.2 9.0 %all-gather.4.cloned.1.call-done = bf16[512,2048]{1,0:T(8,128)(2,1)} async-done(((bf16[512,1024]{1,0:T(8,128)(2,1)}), bf16[512,2048]{1,0:T(8,128)(2,1)}) %all-gather.4.cloned.1.call-update) | async-done | bytes 2097168 | tf_op jit(solution)/shard_map/all_gather | solution.py:131
  56.2 3.8 %select_convert_fusion = (bf16[512,512]{1,0:T(8,128)(2,1)S(1)}, f32[512,512]{1,0:T(8,128)S(1)}) fusion(bf16[1,512,512]{2,1,0:T(8,128)(2,1)S(1)} %copy-done.42, bf16[1,512,512]{2,1,0:T(8,128)(2,1)S(1)} %copy-done.40, bf16[512,2048]{1,0:T(8,128)(2,1)} %all-gather.4.cloned.1.call-done, bf16[1,512,2048]{2,1,0:T(8,128)(2,1)} %param.25), kind=kOutput, calls=%fused_computation.62 | convolution fusion | flops 1077411840 | bytes 6815744 | tf_op jit(solution)/shard_map/rd,fd->rf/dot_general | solution.py:26
  62.3 2.6 %add_convert_fusion = bf16[512,2048]{1,0:T(8,128)(2,1)} fusion(f32[512,2048]{1,0:T(8,128)S(1)} %fusion.4, bf16[512,512]{1,0:T(8,128)(2,1)S(1)} %get-tuple-element.79, bf16[1,2048,512]{2,1,0:T(8,128)(2,1)S(1)} %copy-done.11), kind=kOutput, calls=%fused_computation.1 | convolution fusion | flops 1075838976 | bytes 8912896 | tf_op jit(solution)/shard_map/rf,df->rd/dot_general | solution.py:44
  75.9 7.0 %all-to-all-start.1 = ((bf16[16,32,1024]{2,1,0:T(8,128)(2,1)}), bf16[16,32,1024]{2,1,0:T(8,128)(2,1)}, u32[]{:S(2)}, u32[]{:S(2)}) async-start(bf16[16,32,1024]{2,1,0:T(8,128)(2,1)} %bitcast.217), calls=%async_computation.2 | async-start | bytes 2097152 | tf_op jit(solution)/shard_map/all_to_all | solution.py:142
  83.5 1.7 constant_dynamic-slice_fusion
  85.2 27.8 %all-to-all-done.1 = bf16[16,32,1024]{2,1,0:T(8,128)(2,1)} async-done(((bf16[16,32,1024]{2,1,0:T(8,128)(2,1)}), bf16[16,32,1024]{2,1,0:T(8,128)(2,1)}, u32[]{:S(2)}, u32[]{:S(2)}) %all-to-all-start.1) | async-done | bytes 1048608 | tf_op jit(solution)/shard_map/all_to_all | solution.py:142
  113.7 6.2 %all-to-all-start.4 = ((f32[16,1,16]{2,1,0:T(1,128)}), f32[16,1,16]{2,1,0:T(1,128)}, u32[]{:S(2)}, u32[]{:S(2)}) async-start(f32[16,1,16]{2,1,0:T(1,128)} %broadcast_in_dim.61), calls=%async_computation.5 | async-start | bytes 16384 | tf_op jit(solution)/shard_map/all_to_all | solution.py:51
  121.5 2.2 all_gather.13
  124.5 4.5 %fusion.86 = f32[128,1024]{1,0:T(8,128)} fusion(bf16[128,2048]{1,0:T(8,128)(2,1)S(1)} %all_gather.13, bf16[1024,2048]{1,0:T(8,128)(2,1)} %param.26), kind=kOutput, calls=%fused_computation.145 | convolution fusion | flops 536870912 | bytes 5242880 | tf_op jit(solution)/shard_map/td,id->ti/dot_general | solution.py:214
  129.0 2.1 reshape.254
  131.2 1.7 multiply_reduce_fusion.3
  137.4 6.9 %all-to-all-start.5 = ((bf16[16,64,128]{2,1,0:T(8,128)(2,1)}), bf16[16,64,128]{2,1,0:T(8,128)(2,1)}, u32[]{:S(2)}, u32[]{:S(2)}) async-start(bf16[16,64,128]{2,1,0:T(8,128)(2,1)} %bitcast.216), calls=%async_computation.6 | async-start | bytes 524288 | tf_op jit(solution)/shard_map/all_to_all | solution.py:75
  144.3 2.4 convolution_convert_fusion.3
  146.7 12.2 %all-to-all-done.5 = bf16[16,64,128]{2,1,0:T(8,128)(2,1)} async-done(((bf16[16,64,128]{2,1,0:T(8,128)(2,1)}), bf16[16,64,128]{2,1,0:T(8,128)(2,1)}, u32[]{:S(2)}, u32[]{:S(2)}) %all-to-all-start.5) | async-done | bytes 262176 | tf_op jit(solution)/shard_map/all_to_all | solution.py:75
  158.9 7.2 %all-to-all-start.2 = ((bf16[16,32,1024]{2,1,0:T(8,128)(2,1)}), bf16[16,32,1024]{2,1,0:T(8,128)(2,1)}, u32[]{:S(2)}, u32[]{:S(2)}) async-start(bf16[16,32,1024]{2,1,0:T(8,128)(2,1)} %bitcast.202), calls=%async_computation.3 | async-start | bytes 2097152 | tf_op jit(solution)/shard_map/all_to_all | solution.py:124
  166.6 4.8 %fusion.2 = bf16[1,512,2048]{2,1,0:T(8,128)(2,1)} fusion(bf16[512,2048]{1,0:T(8,128)(2,1)} %all-gather.4.cloned.1.call-done, bf16[1,512,512]{2,1,0:T(8,128)(2,1)} %param.22, bf16[1,512,512]{2,1,0:T(8,128)(2,1)} %param.21), kind=kOutput, calls=%fused_computation.7 | convolution fusion | flops 1077936128 | bytes 5242880 | tf_op jit(solution)/shard_map/rf,rd->fd/dot_general | solution.py:192
  175.7 3.3 %multiply_reduce_fusion = bf16[16,64,128]{2,1,0:T(8,128)(2,1)} fusion(f32[16,64,128]{2,1,0:T(8,128)S(1)} %convert_element_type.168, f32[16,16,64]{2,1,0:T(8,128)S(1)} %fusion.74), kind=kLoop, calls=%fused_computation | loop fusion | flops 4063232 | bytes 851968 | tf_op jit(solution)/shard_map/reduce_sum | solution.py:82
  179.0 10.2 %all-to-all-done.2 = bf16[16,32,1024]{2,1,0:T(8,128)(2,1)} async-done(((bf16[16,32,1024]{2,1,0:T(8,128)(2,1)}), bf16[16,32,1024]{2,1,0:T(8,128)(2,1)}, u32[]{:S(2)}, u32[]{:S(2)}) %all-to-all-start.2) | async-done | bytes 1048608 | tf_op jit(solution)/shard_map/all_to_all | solution.py:124
  189.2 6.0 %all-to-all-start.6 = ((bf16[16,64,128]{2,1,0:T(8,128)(2,1)}), bf16[16,64,128]{2,1,0:T(8,128)(2,1)}, u32[]{:S(2)}, u32[]{:S(2)}) async-start(bf16[16,64,128]{2,1,0:T(8,128)(2,1)} %multiply_reduce_fusion), calls=%async_computation.7 | async-start | bytes 524288 | tf_op jit(solution)/shard_map/all_to_all | solution.py:83
  195.3 1.9 fusion.13
  198.8 2.0 bitcast_bitcast_fusion
  200.9 2.8 %all-to-all-done.6 = bf16[16,64,128]{2,1,0:T(8,128)(2,1)} async-done(((bf16[16,64,128]{2,1,0:T(8,128)(2,1)}), bf16[16,64,128]{2,1,0:T(8,128)(2,1)}, u32[]{:S(2)}, u32[]{:S(2)}) %all-to-all-start.6) | async-done | bytes 262176 | tf_op jit(solution)/shard_map/all_to_all | solution.py:83
  203.8 4.2 %all-to-all-start.3 = ((bf16[16,128,128]{2,1,0:T(8,128)(2,1)}), bf16[16,128,128]{2,1,0:T(8,128)(2,1)}, u32[]{:S(2)}, u32[]{:S(2)}) async-start(bf16[16,128,128]{2,1,0:T(8,128)(2,1)} %bitcast_bitcast_fusion), calls=%async_computation.4 | async-start | bytes 1048576 | tf_op jit(solution)/shard_map/all_to_all | solution.py:201
  209.4 1.8 fusion.12
  215.1 1.8 copy.142
  217.0 4.0 %all-to-all-done.3 = bf16[16,128,128]{2,1,0:T(8,128)(2,1)} async-done(((bf16[16,128,128]{2,1,0:T(8,128)(2,1)}), bf16[16,128,128]{2,1,0:T(8,128)(2,1)}, u32[]{:S(2)}, u32[]{:S(2)}) %all-to-all-start.3) | async-done | bytes 524320 | tf_op jit(solution)/shard_map/all_to_all | solution.py:201
  221.6 3.8 %all-to-all-start.7 = ((f32[16,1,16]{2,1,0:T(1,128)}), f32[16,1,16]{2,1,0:T(1,128)S(1)}, u32[]{:S(2)}, u32[]{:S(2)}) async-start(f32[16,1,16]{2,1,0:T(1,128)} %broadcast_in_dim.100), calls=%async_computation.8 | async-start | bytes 16384 | tf_op jit(solution)/shard_map/all_to_all | solution.py:51
  225.5 3.9 %fusion.85 = f32[128,1024]{1,0:T(8,128)} fusion(bf16[2048,128]{1,0:T(8,128)(2,1)} %bitcast.29, bf16[2048,1024]{1,0:T(8,128)(2,1)} %all-gather.8.cloned.1.call-done), kind=kOutput, calls=%fused_computation.144 | convolution fusion | flops 536870912 | bytes 5242880 | tf_op jit(solution)/shard_map/td,ti->di/dot_general | solution.py:208
  229.5 3.2 %all-to-all-done.7 = f32[16,1,16]{2,1,0:T(1,128)S(1)} async-done(((f32[16,1,16]{2,1,0:T(1,128)}), f32[16,1,16]{2,1,0:T(1,128)S(1)}, u32[]{:S(2)}, u32[]{:S(2)}) %all-to-all-start.7) | async-done | bytes 1056 | tf_op jit(solution)/shard_map/all_to_all | solution.py:51
  233.6 4.4 %fusion.1 = bf16[1,2048,512]{2,1,0:T(8,128)(2,1)} fusion(bf16[512,2048]{1,0:T(8,128)(2,1)} %all-gather.6.cloned.1.call-done, bf16[512,512]{1,0:T(8,128)(2,1)S(1)} %copy-done.21), kind=kOutput, calls=%fused_computation.6 | convolution fusion | flops 1074790400 | bytes 4718592 | tf_op jit(solution)/shard_map/rd,rf->df/dot_general | solution.py:198
  238.0 2.9 %fusion = bf16[1,2048,512]{2,1,0:T(8,128)(2,1)} fusion(bf16[512,2048]{1,0:T(8,128)(2,1)S(1)} %copy-done.39, bf16[1,512,512]{2,1,0:T(8,128)(2,1)S(1)} %copy-done.41, f32[512,512]{1,0:T(8,128)S(1)} %copy-done.45, bf16[1,512,512]{2,1,0:T(8,128)(2,1)S(1)} %copy-done.43), kind=kOutput, calls=%fused_computation.5 | convolution fusion | flops 1079508992 | bytes 6291456 | tf_op jit(solution)/shard_map/rd,rf->df/dot_general | solution.py:195
  (168 shorter events, 39.0 us)
Async XLA Ops:
  8.0 52.1 %copy-start = (bf16[1,2048,512]{2,1,0:T(8,128)(2,1)S(1)}, bf16[1,2048,512]{2,1,0:T(8,128)(2,1)}, u32[]{:S(2)}) copy-start(bf16[1,2048,512]{2,1,0:T(8,128)(2,1)} %param.23) | copy-start | bytes 6291460
  8.0 48.2 %all-gather.4.cloned.1.call-start = ((), (), s32[]{:S(2)}) async-start(), calls=%async_computation.9 | async-start | bytes 3145728 | tf_op jit(solution)/shard_map/all_gather | solution.py:131
  10.3 36.9 %copy-start.31 = (s32[2,128]{1,0:T(2,128)}, s32[2,128]{1,0:T(2,128)S(1)}, u32[]{:S(2)}) copy-start(s32[2,128]{1,0:T(2,128)S(1)} %add_bitcast_fusion) | copy-start | bytes 3076
  11.3 45.0 %copy-start.40 = (bf16[1,512,512]{2,1,0:T(8,128)(2,1)S(1)}, bf16[1,512,512]{2,1,0:T(8,128)(2,1)}, u32[]{:S(2)}) copy-start(bf16[1,512,512]{2,1,0:T(8,128)(2,1)} %param.21) | copy-start | bytes 1572868
  11.3 45.0 %copy-start.42 = (bf16[1,512,512]{2,1,0:T(8,128)(2,1)S(1)}, bf16[1,512,512]{2,1,0:T(8,128)(2,1)}, u32[]{:S(2)}) copy-start(bf16[1,512,512]{2,1,0:T(8,128)(2,1)} %param.22) | copy-start | bytes 1572868
  47.2 28.7 %reduce-scatter.2.cloned.1.call-start = ((), (), s32[]{:S(2)}) async-start(), calls=%async_computation.10 | async-start | bytes 3145728 | tf_op jit(solution)/shard_map/reduce_scatter | solution.py:139
  64.9 160.6 %all-gather.8.cloned.1.call-start = ((), (), s32[]{:S(2)}) async-start(), calls=%async_computation.12 | async-start | bytes 4456448 | tf_op jit(solution)/shard_map/all_gather | solution.py:180
  75.5 7.4 %copy-start.34 = (bf16[1024]{0:T(1024)(128)(2,1)S(1)}, bf16[1024]{0:T(1024)(128)(2,1)}, u32[]{:S(2)}) copy-start(bf16[1024]{0:T(1024)(128)(2,1)} %param.27) | copy-start | bytes 6148
  75.5 8.0 %copy-start.32 = (s32[2,128]{1,0:T(2,128)S(1)}, s32[2,128]{1,0:T(2,128)}, u32[]{:S(2)}) copy-start(s32[2,128]{1,0:T(2,128)} %copy-done.31) | copy-start | bytes 3076
  75.5 37.6 %copy-start.37 = (f32[16]{0:T(128)S(1)}, f32[16]{0:T(128)}, u32[]{:S(2)}) copy-start(f32[16]{0:T(128)} %copy-done.36) | copy-start | bytes 196
  75.9 37.2 %all-to-all-start.1 = ((bf16[16,32,1024]{2,1,0:T(8,128)(2,1)}), bf16[16,32,1024]{2,1,0:T(8,128)(2,1)}, u32[]{:S(2)}, u32[]{:S(2)}) async-start(bf16[16,32,1024]{2,1,0:T(8,128)(2,1)} %bitcast.217), calls=%async_computation.2 | async-start | bytes 2097152 | tf_op jit(solution)/shard_map/all_to_all | solution.py:142
  83.5 40.2 %copy-start.18 = (bf16[512,128]{1,0:T(8,128)(2,1)}, bf16[512,128]{1,0:T(8,128)(2,1)S(1)}, u32[]{:S(2)}) copy-start(bf16[512,128]{1,0:T(8,128)(2,1)S(1)} %fusion.52) | copy-start | bytes 393220
  113.7 23.7 %all-to-all-start.4 = ((f32[16,1,16]{2,1,0:T(1,128)}), f32[16,1,16]{2,1,0:T(1,128)}, u32[]{:S(2)}, u32[]{:S(2)}) async-start(f32[16,1,16]{2,1,0:T(1,128)} %broadcast_in_dim.61), calls=%async_computation.5 | async-start | bytes 16384 | tf_op jit(solution)/shard_map/all_to_all | solution.py:51
  129.0 4.2 %copy-start.5 = (f32[16,8,4,256]{3,1,2,0:T(8,128)S(1)}, f32[16,8,4,256]{3,1,2,0:T(8,128)}, u32[]{:S(2)}) copy-start(f32[16,8,4,256]{3,1,2,0:T(8,128)} %copy-done.4) | copy-start | bytes 1572868
  137.4 21.5 %all-to-all-start.5 = ((bf16[16,64,128]{2,1,0:T(8,128)(2,1)}), bf16[16,64,128]{2,1,0:T(8,128)(2,1)}, u32[]{:S(2)}, u32[]{:S(2)}) async-start(bf16[16,64,128]{2,1,0:T(8,128)(2,1)} %bitcast.216), calls=%async_computation.6 | async-start | bytes 524288 | tf_op jit(solution)/shard_map/all_to_all | solution.py:75
  158.9 30.3 %all-to-all-start.2 = ((bf16[16,32,1024]{2,1,0:T(8,128)(2,1)}), bf16[16,32,1024]{2,1,0:T(8,128)(2,1)}, u32[]{:S(2)}, u32[]{:S(2)}) async-start(bf16[16,32,1024]{2,1,0:T(8,128)(2,1)} %bitcast.202), calls=%async_computation.3 | async-start | bytes 2097152 | tf_op jit(solution)/shard_map/all_to_all | solution.py:124
  166.6 5.9 %copy-start.10 = (bf16[1,16,64,128]{3,2,1,0:T(8,128)(2,1)S(1)}, bf16[1,16,64,128]{3,2,1,0:T(8,128)(2,1)}, u32[]{:S(2)}) copy-start(bf16[1,16,64,128]{3,2,1,0:T(8,128)(2,1)} %copy-done.9) | copy-start | bytes 786436
  166.6 6.9 %copy-start.28 = (pred[128,128]{1,0:T(8,128)(4,1)S(1)}, pred[128,128]{1,0:T(8,128)(4,1)}, u32[]{:S(2)}) copy-start(pred[128,128]{1,0:T(8,128)(4,1)} %copy-done.27) | copy-start | bytes 49156
  173.6 21.7 %copy-start.17 = (bf16[128,4,128]{0,2,1:T(8,128)(2,1)S(1)}, bf16[128,4,128]{0,2,1:T(8,128)(2,1)}, u32[]{:S(2)}) copy-start(bf16[128,4,128]{0,2,1:T(8,128)(2,1)} %copy-done.16) | copy-start | bytes 393220
  189.2 14.6 %all-to-all-start.6 = ((bf16[16,64,128]{2,1,0:T(8,128)(2,1)}), bf16[16,64,128]{2,1,0:T(8,128)(2,1)}, u32[]{:S(2)}, u32[]{:S(2)}) async-start(bf16[16,64,128]{2,1,0:T(8,128)(2,1)} %multiply_reduce_fusion), calls=%async_computation.7 | async-start | bytes 524288 | tf_op jit(solution)/shard_map/all_to_all | solution.py:83
  195.2 38.3 %all-gather.6.cloned.1.call-start = ((), (), s32[]{:S(2)}) async-start(), calls=%async_computation.11 | async-start | bytes 3145728 | tf_op jit(solution)/shard_map/all_gather | solution.py:131
  198.8 9.2 %copy-start.26 = (f32[128,16]{0,1:T(8,128)S(1)}, f32[128,16]{0,1:T(8,128)}, u32[]{:S(2)}) copy-start(f32[128,16]{0,1:T(8,128)} %get-tuple-element.77) | copy-start | bytes 24580
  200.9 12.0 %copy-start.14 = (bf16[128,4,128]{2,1,0:T(4,128)(2,1)S(1)}, bf16[128,4,128]{2,1,0:T(4,128)(2,1)}, u32[]{:S(2)}) copy-start(bf16[128,4,128]{2,1,0:T(4,128)(2,1)} %copy-done.13) | copy-start | bytes 393220
  203.8 17.2 %all-to-all-start.3 = ((bf16[16,128,128]{2,1,0:T(8,128)(2,1)}), bf16[16,128,128]{2,1,0:T(8,128)(2,1)}, u32[]{:S(2)}, u32[]{:S(2)}) async-start(bf16[16,128,128]{2,1,0:T(8,128)(2,1)} %bitcast_bitcast_fusion), calls=%async_computation.4 | async-start | bytes 1048576 | tf_op jit(solution)/shard_map/all_to_all | solution.py:201
  208.0 6.1 %copy-start.3 = (bf16[16,128,128]{2,1,0:T(8,128)(2,1)S(1)}, bf16[16,128,128]{2,1,0:T(8,128)(2,1)}, u32[]{:S(2)}) copy-start(bf16[16,128,128]{2,1,0:T(8,128)(2,1)} %copy-done.2) | copy-start | bytes 1572868
  221.6 11.1 %all-to-all-start.7 = ((f32[16,1,16]{2,1,0:T(1,128)}), f32[16,1,16]{2,1,0:T(1,128)S(1)}, u32[]{:S(2)}, u32[]{:S(2)}) async-start(f32[16,1,16]{2,1,0:T(1,128)} %broadcast_in_dim.100), calls=%async_computation.8 | async-start | bytes 16384 | tf_op jit(solution)/shard_map/all_to_all | solution.py:51
  225.5 7.2 %copy-start.38 = (pred[16]{0:T(512)(128)(4,1)S(1)}, pred[16]{0:T(512)(128)(4,1)}, u32[]{:S(2)}) copy-start(pred[16]{0:T(512)(128)(4,1)} %iota_compare_fusion.11) | copy-start | bytes 52
  225.5 8.0 %copy-start.21 = (bf16[512,512]{1,0:T(8,128)(2,1)S(1)}, bf16[512,512]{1,0:T(8,128)(2,1)}, u32[]{:S(2)}) copy-start(bf16[512,512]{1,0:T(8,128)(2,1)} %copy-done.20) | copy-start | bytes 1572868
  233.6 4.4 %copy-start.41 = (bf16[1,512,512]{2,1,0:T(8,128)(2,1)S(1)}, bf16[1,512,512]{2,1,0:T(8,128)(2,1)}, u32[]{:S(2)}) copy-start(bf16[1,512,512]{2,1,0:T(8,128)(2,1)} %param.21) | copy-start | bytes 1572868
  233.6 4.4 %copy-start.39 = (bf16[512,2048]{1,0:T(8,128)(2,1)S(1)}, bf16[512,2048]{1,0:T(8,128)(2,1)}, u32[]{:S(2)}) copy-start(bf16[512,2048]{1,0:T(8,128)(2,1)} %all-gather.6.cloned.1.call-done) | copy-start | bytes 6291460
  233.6 4.4 %copy-start.43 = (bf16[1,512,512]{2,1,0:T(8,128)(2,1)S(1)}, bf16[1,512,512]{2,1,0:T(8,128)(2,1)}, u32[]{:S(2)}) copy-start(bf16[1,512,512]{2,1,0:T(8,128)(2,1)} %param.22) | copy-start | bytes 1572868
  233.6 4.4 %copy-start.45 = (f32[512,512]{1,0:T(8,128)S(1)}, f32[512,512]{1,0:T(8,128)}, u32[]{:S(2)}) copy-start(f32[512,512]{1,0:T(8,128)} %copy-done.44) | copy-start | bytes 3145732
  (25 other events, 41.9 us)
Sparse Core Ops, SparseCore 0:
  47.3 8.8 all-gather.3
  65.0 10.7 reduce-scatter.1
Sparse Core Ops, SparseCore 1:
  75.6 89.1 all-gather.7
  200.9 11.7 all-gather.5
where the time goes:
time: 250 us; the launch traced here: 248 us
  waiting for transfers between devices  69.7 us (28%)
  matrix products  47.4 us (19%)
  starting transfers between devices  41.5 us (17%)
  blocking collectives  36.7 us (15%)
  local copies, waits for them, and re-layouts  21.3 us (9%)
  between operations  16.3 us (7%)
  other arithmetic  15.4 us (6%)
    all_to_all x1, blocking collectives, dispatch(): lax.all_to_all(rows.astype(jnp.bfloat16).reshape(expert_count, capacity,...  34.6 us
    all_to_all x1, waiting for transfers between devices, body(): lax.all_to_all(summed.reshape(expert_count, capacity, -1), 'sp', split_ax...  27.8 us
    all_to_all x1, waiting for transfers between devices, later_states(): lax.all_to_all(block_state.astype(jnp.bfloat16).reshape(count, rows, widt...  12.2 us
    all_to_all x1, waiting for transfers between devices, dispatch(): lax.all_to_all(rows.astype(jnp.bfloat16).reshape(expert_count, capacity,...  10.2 us
    all_to_all x2, starting transfers between devices, exchange(): return lax.all_to_all(pieces, 'sp', split_axis=0, concat_axis=0, tiled=True)  10.1 us
    unnamed x99, local copies, waits for them, and re-layouts  9.1 us
    all_gather x2, waiting for transfers between devices, dispatch(): return lax.all_gather(arrived, 'tp', axis=1, tiled=True)  9.01 us
    all_to_all x1, starting transfers between devices, dispatch(): lax.all_to_all(rows.astype(jnp.bfloat16).reshape(expert_count, capacity,...  7.18 us
  transfers between devices with their start and end apart: 11, of which 8 were waited for; matrix products, arithmetic and copies ran while one was open for 25% of the time, Pallas kernels for 0%

commit v1 on v0

--- a/solution.py
+++ b/solution.py
@@ -128,7 +128,9 @@
             concat_axis=0,
             tiled=True,
         ).reshape(-1, columns)
-        return lax.all_gather(arrived, "tp", axis=1, tiled=True)
+        return jnp.concatenate(
+            lax.all_to_all(jnp.stack([arrived] * lax.axis_size("tp")), "tp", 0, 0), axis=1
+        )
 
     recv_grads = dispatch(
         jnp.einsum("kst,ktd->sd", places, weighted, preferred_element_type=jnp.float32)

time: 250 us -> 259 us (1.036)
  blocking collectives: 36.7 us -> 49.5 us
  matrix products: 47.4 us -> 39.3 us
  waiting for transfers between devices: 69.7 us -> 76.8 us
  starting transfers between devices: 41.5 us -> 38.2 us
    all_to_all x0 -> x2, blocking collectives: none -> 12.6 us  [dispatch(): lax.all_to_all(jnp.stack([arrived] * lax.axis_size('tp')), 'tp', 0, 0)]
    all_to_all x1, waiting for transfers between devices: 4.01 us -> 13.3 us  [body(): lax.all_to_all(grad_hidden.reshape(tokens_here, expert_count, -1).transpo...]
    all_gather x2 -> x0, waiting for transfers between devices: 9.01 us -> none  [dispatch(): return lax.all_gather(arrived, 'tp', axis=1, tiled=True)]
    all_to_all x1, waiting for transfers between devices: 2.84 us -> 9.82 us  [later_states(): lax.all_to_all(sums.astype(jnp.bfloat16), 'sp', split_axis=0, concat_axis...]
    reshape x0 -> x2, local copies, waits for them, and re-layouts: none -> 6.94 us  [dispatch(): jnp.concatenate(lax.all_to_all(jnp.stack([arrived] * lax.axis_size('tp'))...]
    all_to_all x1, starting transfers between devices: 7.18 us -> 3.66 us  [dispatch(): lax.all_to_all(rows.astype(jnp.bfloat16).reshape(expert_count, capacity,...]
    all_to_all x1, waiting for transfers between devices: 27.8 us -> 25.1 us  [body(): lax.all_to_all(summed.reshape(expert_count, capacity, -1), 'sp', split_ax...]
    unnamed x99 -> x117, local copies, waits for them, and re-layouts: 9.1 us -> 7.99 us
  transfers between devices with their start and end apart: 11 -> 9, of which waited for: 8 -> 7; matrix products, arithmetic and copies ran while one was open for 25% -> 18% of each run, Pallas kernels for 0% -> 0%
where the time goes in v1:
time: 259 us; the launch traced here: 257 us
  waiting for transfers between devices  76.8 us (30%)
  blocking collectives  49.5 us (19%)
  matrix products  39.3 us (15%)
  starting transfers between devices  38.2 us (15%)
  local copies, waits for them, and re-layouts  22.7 us (9%)
  between operations  16.3 us (6%)
  other arithmetic  14.7 us (6%)
    all_to_all x1, blocking collectives, dispatch(): lax.all_to_all(rows.astype(jnp.bfloat16).reshape(expert_count, capacity,...  34.5 us
    all_to_all x1, waiting for transfers between devices, body(): lax.all_to_all(summed.reshape(expert_count, capacity, -1), 'sp', split_ax...  25.1 us
    all_to_all x1, waiting for transfers between devices, later_states(): lax.all_to_all(block_state.astype(jnp.bfloat16).reshape(count, rows, widt...  13.6 us
    all_to_all x1, waiting for transfers between devices, body(): lax.all_to_all(grad_hidden.reshape(tokens_here, expert_count, -1).transpo...  13.3 us
    all_to_all x2, blocking collectives, dispatch(): lax.all_to_all(jnp.stack([arrived] * lax.axis_size('tp')), 'tp', 0, 0)  12.6 us
    all_to_all x2, starting transfers between devices, exchange(): return lax.all_to_all(pieces, 'sp', split_axis=0, concat_axis=0, tiled=True)  10 us
    all_to_all x1, waiting for transfers between devices, later_states(): lax.all_to_all(sums.astype(jnp.bfloat16), 'sp', split_axis=0, concat_axis...  9.82 us
    all_to_all x1, waiting for transfers between devices, dispatch(): lax.all_to_all(rows.astype(jnp.bfloat16).reshape(expert_count, capacity,...  9.22 us
  transfers between devices with their start and end apart: 9, of which 7 were waited for; matrix products, arithmetic and copies ran while one was open for 18% of the time, Pallas kernels for 0%

profile of v1, /device:TPU:0, one launch (start us, length us, event | category | flops | bytes accessed | tf_op | source)
XLA Modules:
  0.0 257.5 jit_solution(9731911924186246986)
XLA Ops:
  12.5 34.5 %all_to_all.58 = bf16[16,32,1024]{2,1,0:T(8,128)(2,1)S(1)} all-to-all(bf16[16,32,1024]{2,1,0:T(8,128)(2,1)S(1)} %bitcast.209), channel_id=1, replica_groups=mesh['sp'=16,'tp'=2] {'sp'}, dimensions={0} | all-to-all | bytes 2097152 | tf_op jit(solution)/shard_map/all_to_all | solution.py:124
  47.1 6.3 %all_to_all.59 = bf16[2,512,1024]{2,1,0:T(8,128)(2,1)} all-to-all(bf16[2,512,1024]{2,1,0:T(8,128)(2,1)S(1)} %pad_maximum_fusion), channel_id=1, replica_groups=mesh['sp'=16,'tp'=2] {'tp'}, dimensions={0} | all-to-all | bytes 4194304 | tf_op jit(solution)/shard_map/all_to_all | solution.py:132
  53.4 4.0 %copy.136 = bf16[512,2,1024]{0,2,1:T(8,128)(2,1)} copy(bf16[512,2,1024]{2,0,1:T(8,128)(2,1)} %bitcast.202) | data formatting | bytes 4194304 | tf_op jit(solution)/shard_map/reshape | solution.py:131
  57.5 3.8 %fusion.33 = (bf16[512,512]{1,0:T(8,128)(2,1)S(1)}, f32[512,512]{1,0:T(8,128)S(1)}) fusion(bf16[1,512,512]{2,1,0:T(8,128)(2,1)S(1)} %copy-done.47, bf16[1,512,512]{2,1,0:T(8,128)(2,1)S(1)} %copy-done.50, bf16[512,2048]{0,1:T(8,128)(2,1)} %bitcast.220, bf16[1,512,2048]{2,1,0:T(8,128)(2,1)} %param.25), kind=kOutput, calls=%fused_computation.59 | convolution fusion | flops 1077411840 | bytes 6815744 | tf_op jit(solution)/shard_map/rd,fd->rf/dot_general | solution.py:26
  61.4 1.7 fusion.4
  63.5 2.6 %add_convert_fusion = bf16[512,2048]{1,0:T(8,128)(2,1)} fusion(f32[512,2048]{1,0:T(8,128)S(1)} %fusion.4, bf16[512,512]{1,0:T(8,128)(2,1)S(1)} %get-tuple-element.79, bf16[1,2048,512]{2,1,0:T(8,128)(2,1)S(1)} %copy-done.8), kind=kOutput, calls=%fused_computation.1 | convolution fusion | flops 1075838976 | bytes 8912896 | tf_op jit(solution)/shard_map/rf,df->rd/dot_general | solution.py:44
  74.3 7.1 %all-to-all-start.2 = ((bf16[16,32,1024]{2,1,0:T(8,128)(2,1)}), bf16[16,32,1024]{2,1,0:T(8,128)(2,1)}, u32[]{:S(2)}, u32[]{:S(2)}) async-start(bf16[16,32,1024]{2,1,0:T(8,128)(2,1)} %bitcast.228), calls=%async_computation.3 | async-start | bytes 2097152 | tf_op jit(solution)/shard_map/all_to_all | solution.py:144
  81.4 1.7 multiply_convert_fusion.3
  86.5 25.1 %all-to-all-done.2 = bf16[16,32,1024]{2,1,0:T(8,128)(2,1)} async-done(((bf16[16,32,1024]{2,1,0:T(8,128)(2,1)}), bf16[16,32,1024]{2,1,0:T(8,128)(2,1)}, u32[]{:S(2)}, u32[]{:S(2)}) %all-to-all-start.2) | async-done | bytes 1048608 | tf_op jit(solution)/shard_map/all_to_all | solution.py:144
  112.9 6.1 %all-to-all-start.6 = ((f32[16,1,16]{2,1,0:T(1,128)}), f32[16,1,16]{2,1,0:T(1,128)}, u32[]{:S(2)}, u32[]{:S(2)}) async-start(f32[16,1,16]{2,1,0:T(1,128)} %broadcast_in_dim.61), calls=%async_computation.7 | async-start | bytes 16384 | tf_op jit(solution)/shard_map/all_to_all | solution.py:51
  119.0 1.6 fusion.15
  120.6 2.4 all_gather.6
  122.9 3.7 %fusion.95 = f32[128,1024]{1,0:T(8,128)S(1)} fusion(bf16[128,2048]{1,0:T(8,128)(2,1)S(1)} %all_gather.6, bf16[1024,2048]{1,0:T(8,128)(2,1)} %param.26), kind=kOutput, calls=%fused_computation.156 | convolution fusion | flops 536870912 | bytes 5242880 | tf_op jit(solution)/shard_map/td,id->ti/dot_general | solution.py:216
  127.7 1.5 multiply_reduce_fusion.3
  131.9 6.9 %all-to-all-start.7 = ((bf16[16,64,128]{2,1,0:T(8,128)(2,1)}), bf16[16,64,128]{2,1,0:T(8,128)(2,1)S(1)}, u32[]{:S(2)}, u32[]{:S(2)}) async-start(bf16[16,64,128]{2,1,0:T(8,128)(2,1)} %bitcast.43), calls=%async_computation.8 | async-start | bytes 524288 | tf_op jit(solution)/shard_map/all_to_all | solution.py:75
  139.9 13.6 %all-to-all-done.7 = bf16[16,64,128]{2,1,0:T(8,128)(2,1)S(1)} async-done(((bf16[16,64,128]{2,1,0:T(8,128)(2,1)}), bf16[16,64,128]{2,1,0:T(8,128)(2,1)S(1)}, u32[]{:S(2)}, u32[]{:S(2)}) %all-to-all-start.7) | async-done | bytes 262176 | tf_op jit(solution)/shard_map/all_to_all | solution.py:75
  153.6 3.3 %multiply_reduce_fusion = bf16[16,64,128]{2,1,0:T(8,128)(2,1)} fusion(f32[16,64,128]{2,1,0:T(8,128)S(1)} %convert_element_type.174, f32[16,16,64]{2,1,0:T(8,128)S(1)} %fusion.83), kind=kLoop, calls=%fused_computation | loop fusion | flops 4063232 | bytes 851968 | tf_op jit(solution)/shard_map/reduce_sum | solution.py:82
  156.8 6.9 %all-to-all-start.8 = ((bf16[16,64,128]{2,1,0:T(8,128)(2,1)}), bf16[16,64,128]{2,1,0:T(8,128)(2,1)S(1)}, u32[]{:S(2)}, u32[]{:S(2)}) async-start(bf16[16,64,128]{2,1,0:T(8,128)(2,1)} %multiply_reduce_fusion), calls=%async_computation.9 | async-start | bytes 524288 | tf_op jit(solution)/shard_map/all_to_all | solution.py:83
  165.3 9.8 %all-to-all-done.8 = bf16[16,64,128]{2,1,0:T(8,128)(2,1)S(1)} async-done(((bf16[16,64,128]{2,1,0:T(8,128)(2,1)}), bf16[16,64,128]{2,1,0:T(8,128)(2,1)S(1)}, u32[]{:S(2)}, u32[]{:S(2)}) %all-to-all-start.8) | async-done | bytes 262176 | tf_op jit(solution)/shard_map/all_to_all | solution.py:83
  175.1 3.6 %all-to-all-start.5 = ((bf16[16,128,128]{2,1,0:T(8,128)(2,1)}), bf16[16,128,128]{2,1,0:T(8,128)(2,1)S(1)}, u32[]{:S(2)}, u32[]{:S(2)}) async-start(bf16[16,128,128]{2,1,0:T(8,128)(2,1)} %bitcast_bitcast_fusion), calls=%async_computation.6 | async-start | bytes 1048576 | tf_op jit(solution)/shard_map/all_to_all | solution.py:203
  180.2 13.3 %all-to-all-done.5 = bf16[16,128,128]{2,1,0:T(8,128)(2,1)S(1)} async-done(((bf16[16,128,128]{2,1,0:T(8,128)(2,1)}), bf16[16,128,128]{2,1,0:T(8,128)(2,1)S(1)}, u32[]{:S(2)}, u32[]{:S(2)}) %all-to-all-start.5) | async-done | bytes 524320 | tf_op jit(solution)/shard_map/all_to_all | solution.py:203
  194.1 3.9 %all-to-all-start.9 = ((f32[16,1,16]{2,1,0:T(1,128)}), f32[16,1,16]{2,1,0:T(1,128)S(1)}, u32[]{:S(2)}, u32[]{:S(2)}) async-start(f32[16,1,16]{2,1,0:T(1,128)} %broadcast_in_dim.100), calls=%async_computation.10 | async-start | bytes 16384 | tf_op jit(solution)/shard_map/all_to_all | solution.py:51
  198.1 2.3 convolution_convert_fusion.3
  200.4 4.9 %all-to-all-done.9 = f32[16,1,16]{2,1,0:T(1,128)S(1)} async-done(((f32[16,1,16]{2,1,0:T(1,128)}), f32[16,1,16]{2,1,0:T(1,128)S(1)}, u32[]{:S(2)}, u32[]{:S(2)}) %all-to-all-start.9) | async-done | bytes 1056 | tf_op jit(solution)/shard_map/all_to_all | solution.py:51
  205.9 3.7 %all-to-all-start.3 = ((bf16[16,32,1024]{2,1,0:T(8,128)(2,1)}), bf16[16,32,1024]{2,1,0:T(8,128)(2,1)S(1)}, u32[]{:S(2)}, u32[]{:S(2)}) async-start(bf16[16,32,1024]{2,1,0:T(8,128)(2,1)} %bitcast.25), calls=%async_computation.4 | async-start | bytes 2097152 | tf_op jit(solution)/shard_map/all_to_all | solution.py:124
  209.6 4.6 %fusion.2 = bf16[1,512,2048]{2,1,0:T(8,128)(2,1)} fusion(bf16[512,2048]{0,1:T(8,128)(2,1)} %bitcast.221, bf16[1,512,512]{2,1,0:T(8,128)(2,1)S(1)} %copy-done.48, bf16[1,512,512]{2,1,0:T(8,128)(2,1)S(1)} %copy-done.51), kind=kOutput, calls=%fused_computation.7 | convolution fusion | flops 1077936128 | bytes 5242880 | tf_op jit(solution)/shard_map/rf,rd->fd/dot_general | solution.py:194
  218.2 3.7 %fusion.94 = f32[128,1024]{1,0:T(8,128)} fusion(bf16[2048,128]{1,0:T(8,128)(2,1)S(1)} %bitcast.217, bf16[2048,1024]{1,0:T(8,128)(2,1)} %all-gather.2.cloned.1.call-done), kind=kOutput, calls=%fused_computation.155 | convolution fusion | flops 536870912 | bytes 5242880 | tf_op jit(solution)/shard_map/td,ti->di/dot_general | solution.py:210
  222.8 9.2 %all-to-all-done.3 = bf16[16,32,1024]{2,1,0:T(8,128)(2,1)S(1)} async-done(((bf16[16,32,1024]{2,1,0:T(8,128)(2,1)}), bf16[16,32,1024]{2,1,0:T(8,128)(2,1)S(1)}, u32[]{:S(2)}, u32[]{:S(2)}) %all-to-all-start.3) | async-done | bytes 1048608 | tf_op jit(solution)/shard_map/all_to_all | solution.py:124
  232.2 6.3 %all_to_all.60 = bf16[2,512,1024]{2,1,0:T(8,128)(2,1)} all-to-all(bf16[2,512,1024]{2,1,0:T(8,128)(2,1)S(1)} %pad_maximum_fusion.1), channel_id=1, replica_groups=mesh['sp'=16,'tp'=2] {'tp'}, dimensions={0} | all-to-all | bytes 4194304 | tf_op jit(solution)/shard_map/all_to_all | solution.py:132
  238.6 2.9 %copy.142 = bf16[512,2,1024]{0,2,1:T(8,128)(2,1)S(1)} copy(bf16[512,2,1024]{2,0,1:T(8,128)(2,1)} %bitcast.203) | data formatting | bytes 4194304 | tf_op jit(solution)/shard_map/reshape | solution.py:131
  242.8 2.6 fusion.1
  245.4 4.6 %fusion = bf16[1,2048,512]{2,1,0:T(8,128)(2,1)} fusion(bf16[512,2048]{0,1:T(8,128)(2,1)} %bitcast.223, bf16[1,512,512]{2,1,0:T(8,128)(2,1)S(1)} %copy-done.49, f32[512,512]{1,0:T(8,128)S(1)} %copy-done.54, bf16[1,512,512]{2,1,0:T(8,128)(2,1)S(1)} %copy-done.52), kind=kOutput, calls=%fused_computation.5 | convolution fusion | flops 1079508992 | bytes 6291456 | tf_op jit(solution)/shard_map/rd,rf->df/dot_general | solution.py:197
  (186 shorter events, 33.0 us)
Async XLA Ops:
  8.0 53.3 %copy-start = (bf16[1,2048,512]{2,1,0:T(8,128)(2,1)S(1)}, bf16[1,2048,512]{2,1,0:T(8,128)(2,1)}, u32[]{:S(2)}) copy-start(bf16[1,2048,512]{2,1,0:T(8,128)(2,1)} %param.23) | copy-start | bytes 6291460
  8.0 66.2 %reduce-scatter.2.cloned.1.call-start = ((), (), s32[]{:S(2)}) async-start(), calls=%async_computation.11 | async-start | bytes 3145728 | tf_op jit(solution)/shard_map/reduce_scatter | solution.py:141
  10.3 36.7 %copy-start.41 = (s32[2,128]{1,0:T(2,128)}, s32[2,128]{1,0:T(2,128)S(1)}, u32[]{:S(2)}) copy-start(s32[2,128]{1,0:T(2,128)S(1)} %add_bitcast_fusion) | copy-start | bytes 3076
  53.4 4.0 %copy-start.47 = (bf16[1,512,512]{2,1,0:T(8,128)(2,1)S(1)}, bf16[1,512,512]{2,1,0:T(8,128)(2,1)}, u32[]{:S(2)}) copy-start(bf16[1,512,512]{2,1,0:T(8,128)(2,1)} %param.21) | copy-start | bytes 1572868
  53.4 4.0 %copy-start.50 = (bf16[1,512,512]{2,1,0:T(8,128)(2,1)S(1)}, bf16[1,512,512]{2,1,0:T(8,128)(2,1)}, u32[]{:S(2)}) copy-start(bf16[1,512,512]{2,1,0:T(8,128)(2,1)} %param.22) | copy-start | bytes 1572868
  74.3 11.5 %copy-start.27 = (bf16[128,2048]{1,0:T(8,128)(2,1)S(1)}, bf16[128,2048]{1,0:T(8,128)(2,1)}, u32[]{:S(2)}) copy-start(bf16[128,2048]{1,0:T(8,128)(2,1)} %param.17) | copy-start | bytes 1572868
  74.3 37.3 %all-to-all-start.2 = ((bf16[16,32,1024]{2,1,0:T(8,128)(2,1)}), bf16[16,32,1024]{2,1,0:T(8,128)(2,1)}, u32[]{:S(2)}, u32[]{:S(2)}) async-start(bf16[16,32,1024]{2,1,0:T(8,128)(2,1)} %bitcast.228), calls=%async_computation.3 | async-start | bytes 2097152 | tf_op jit(solution)/shard_map/all_to_all | solution.py:144
  81.4 136.8 %all-gather.2.cloned.1.call-start = ((), (), s32[]{:S(2)}) async-start(), calls=%async_computation.12 | async-start | bytes 4456448 | tf_op jit(solution)/shard_map/all_gather | solution.py:182
  85.7 33.2 %copy-start.19 = (bf16[512,128]{1,0:T(8,128)(2,1)}, bf16[512,128]{1,0:T(8,128)(2,1)S(1)}, u32[]{:S(2)}) copy-start(bf16[512,128]{1,0:T(8,128)(2,1)S(1)} %fusion.62) | copy-start | bytes 393220
  112.9 19.0 %all-to-all-start.6 = ((f32[16,1,16]{2,1,0:T(1,128)}), f32[16,1,16]{2,1,0:T(1,128)}, u32[]{:S(2)}, u32[]{:S(2)}) async-start(f32[16,1,16]{2,1,0:T(1,128)} %broadcast_in_dim.61), calls=%async_computation.7 | async-start | bytes 16384 | tf_op jit(solution)/shard_map/all_to_all | solution.py:51
  130.6 8.2 %copy-start.42 = (pred[16,16]{1,0:T(8,128)(4,1)S(1)}, pred[16,16]{1,0:T(8,128)(4,1)}, u32[]{:S(2)}) copy-start(pred[16,16]{1,0:T(8,128)(4,1)} %get-tuple-element.82) | copy-start | bytes 772
  130.6 8.2 %copy-start.43 = (pred[16,16]{1,0:T(8,128)(4,1)S(1)}, pred[16,16]{1,0:T(8,128)(4,1)}, u32[]{:S(2)}) copy-start(pred[16,16]{1,0:T(8,128)(4,1)} %get-tuple-element.83) | copy-start | bytes 772
  131.9 21.6 %all-to-all-start.7 = ((bf16[16,64,128]{2,1,0:T(8,128)(2,1)}), bf16[16,64,128]{2,1,0:T(8,128)(2,1)S(1)}, u32[]{:S(2)}, u32[]{:S(2)}) async-start(bf16[16,64,128]{2,1,0:T(8,128)(2,1)} %bitcast.43), calls=%async_computation.8 | async-start | bytes 524288 | tf_op jit(solution)/shard_map/all_to_all | solution.py:75
  153.6 25.2 %copy-start.14 = (bf16[128,4,128]{2,1,0:T(4,128)(2,1)S(1)}, bf16[128,4,128]{2,1,0:T(4,128)(2,1)}, u32[]{:S(2)}) copy-start(bf16[128,4,128]{2,1,0:T(4,128)(2,1)} %copy-done.13) | copy-start | bytes 393220
  156.8 18.2 %all-to-all-start.8 = ((bf16[16,64,128]{2,1,0:T(8,128)(2,1)}), bf16[16,64,128]{2,1,0:T(8,128)(2,1)S(1)}, u32[]{:S(2)}, u32[]{:S(2)}) async-start(bf16[16,64,128]{2,1,0:T(8,128)(2,1)} %multiply_reduce_fusion), calls=%async_computation.9 | async-start | bytes 524288 | tf_op jit(solution)/shard_map/all_to_all | solution.py:83
  163.8 15.2 %copy-start.30 = (f32[128,16]{0,1:T(8,128)S(1)}, f32[128,16]{0,1:T(8,128)}, u32[]{:S(2)}) copy-start(f32[128,16]{0,1:T(8,128)} %get-tuple-element.77) | copy-start | bytes 24580
  175.1 18.4 %all-to-all-start.5 = ((bf16[16,128,128]{2,1,0:T(8,128)(2,1)}), bf16[16,128,128]{2,1,0:T(8,128)(2,1)S(1)}, u32[]{:S(2)}, u32[]{:S(2)}) async-start(bf16[16,128,128]{2,1,0:T(8,128)(2,1)} %bitcast_bitcast_fusion), calls=%async_computation.6 | async-start | bytes 1048576 | tf_op jit(solution)/shard_map/all_to_all | solution.py:203
  178.7 21.7 %copy-start.35 = (f32[128,16]{0,1:T(8,128)}, f32[128,16]{0,1:T(8,128)S(1)}, u32[]{:S(2)}) copy-start(f32[128,16]{0,1:T(8,128)S(1)} %multiply_reduce_fusion.2) | copy-start | bytes 24580
  178.8 19.3 %copy-start.20 = (bf16[512,128]{1,0:T(8,128)(2,1)S(1)}, bf16[512,128]{1,0:T(8,128)(2,1)}, u32[]{:S(2)}) copy-start(bf16[512,128]{1,0:T(8,128)(2,1)} %copy-done.19) | copy-start | bytes 393220
  180.1 25.2 %copy-start.37 = (f32[128,16]{0,1:T(8,128)}, f32[128,16]{0,1:T(8,128)S(1)}, u32[]{:S(2)}) copy-start(f32[128,16]{0,1:T(8,128)S(1)} %get-tuple-element.75) | copy-start | bytes 24580
  180.1 29.5 %copy-start.48 = (bf16[1,512,512]{2,1,0:T(8,128)(2,1)S(1)}, bf16[1,512,512]{2,1,0:T(8,128)(2,1)}, u32[]{:S(2)}) copy-start(bf16[1,512,512]{2,1,0:T(8,128)(2,1)} %param.21) | copy-start | bytes 1572868
  180.1 29.5 %copy-start.51 = (bf16[1,512,512]{2,1,0:T(8,128)(2,1)S(1)}, bf16[1,512,512]{2,1,0:T(8,128)(2,1)}, u32[]{:S(2)}) copy-start(bf16[1,512,512]{2,1,0:T(8,128)(2,1)} %param.22) | copy-start | bytes 1572868
  193.5 11.8 %copy-start.9 = (bf16[16,128,128]{2,1,0:T(8,128)(2,1)}, bf16[16,128,128]{2,1,0:T(8,128)(2,1)S(1)}, u32[]{:S(2)}) copy-start(bf16[16,128,128]{2,1,0:T(8,128)(2,1)S(1)} %all-to-all-done.5) | copy-start | bytes 1572868
  194.1 11.2 %all-to-all-start.9 = ((f32[16,1,16]{2,1,0:T(1,128)}), f32[16,1,16]{2,1,0:T(1,128)S(1)}, u32[]{:S(2)}, u32[]{:S(2)}) async-start(f32[16,1,16]{2,1,0:T(1,128)} %broadcast_in_dim.100), calls=%async_computation.10 | async-start | bytes 16384 | tf_op jit(solution)/shard_map/all_to_all | solution.py:51
  205.9 26.1 %all-to-all-start.3 = ((bf16[16,32,1024]{2,1,0:T(8,128)(2,1)}), bf16[16,32,1024]{2,1,0:T(8,128)(2,1)S(1)}, u32[]{:S(2)}, u32[]{:S(2)}) async-start(bf16[16,32,1024]{2,1,0:T(8,128)(2,1)} %bitcast.25), calls=%async_computation.4 | async-start | bytes 2097152 | tf_op jit(solution)/shard_map/all_to_all | solution.py:124
  209.6 4.6 %copy-start.7 = (bf16[1,16,64,128]{3,2,1,0:T(8,128)(2,1)S(1)}, bf16[1,16,64,128]{3,2,1,0:T(8,128)(2,1)}, u32[]{:S(2)}) copy-start(bf16[1,16,64,128]{3,2,1,0:T(8,128)(2,1)} %copy-done.6) | copy-start | bytes 786436
  209.6 4.9 %copy-start.33 = (pred[128,128]{1,0:T(8,128)(4,1)S(1)}, pred[128,128]{1,0:T(8,128)(4,1)}, u32[]{:S(2)}) copy-start(pred[128,128]{1,0:T(8,128)(4,1)} %copy-done.32) | copy-start | bytes 49156
  218.2 3.8 %copy-start.46 = (pred[16]{0:T(512)(128)(4,1)S(1)}, pred[16]{0:T(512)(128)(4,1)}, u32[]{:S(2)}) copy-start(pred[16]{0:T(512)(128)(4,1)} %iota_compare_fusion.11) | copy-start | bytes 52
  218.2 3.9 %copy-start.36 = (f32[128,16]{0,1:T(8,128)S(1)}, f32[128,16]{0,1:T(8,128)}, u32[]{:S(2)}) copy-start(f32[128,16]{0,1:T(8,128)} %copy-done.35) | copy-start | bytes 24580
  218.2 3.9 %copy-start.38 = (f32[128,16]{0,1:T(8,128)S(1)}, f32[128,16]{0,1:T(8,128)}, u32[]{:S(2)}) copy-start(f32[128,16]{0,1:T(8,128)} %copy-done.37) | copy-start | bytes 24580
  238.5 4.3 %copy-start.24 = (bf16[512,512]{1,0:T(8,128)(2,1)S(1)}, bf16[512,512]{1,0:T(8,128)(2,1)}, u32[]{:S(2)}) copy-start(bf16[512,512]{1,0:T(8,128)(2,1)} %copy-done.23) | copy-start | bytes 1572868
  245.4 4.6 %copy-start.1 = (bf16[1,2048,512]{2,1,0:T(8,128)(2,1)S(1)}, bf16[1,2048,512]{2,1,0:T(8,128)(2,1)}, u32[]{:S(2)}) copy-start(bf16[1,2048,512]{2,1,0:T(8,128)(2,1)} %param.23) | copy-start | bytes 6291460
  (32 other events, 61.3 us)
Sparse Core Ops, SparseCore 0:
  66.3 7.9 reduce-scatter.1
Sparse Core Ops, SparseCore 1:
  84.6 87.4 all-gather.1
